TPU v7x, 32 devices: a whole 2x2x4 slice. The times are simulated.
32 devices in a mesh: ep: 8 (over z, y), tp: 4 (over x, core).
Axes of the slice: x: 2, y: 2, z: 4, core: 2. Of those that a mesh axis runs over, the one named last changes fastest.
Arguments:
- tokens: bfloat16 [2048, 2048], P('ep'), may hold values from -6 to 6
- expert_ids: int32 [2048, 2], P('ep'), may hold values from 0 to 7, all different within a row; in each aligned block of 256 rows (0 to 255, 256 to 511, ...) at most 192 rows name the same one
- route_weight: float32 [2048, 2], P('ep'), may hold values from 0.1 to 1
- norm_gain: float32 [2048], replicated, may hold values from 0.1 to 1.9
- expert_gate: bfloat16 [8, 2048, 2048], P('ep', None, 'tp'), may hold values from -4 to 4
- expert_up: bfloat16 [8, 2048, 2048], P('ep', None, 'tp'), may hold values from -4 to 4
- expert_down: bfloat16 [8, 2048, 2048], P('ep', 'tp'), may hold values from -0.03125 to 0.03125
Outputs:
- combined: bfloat16 [2048, 2048], P('ep', 'tp')
Inputs may be any that keep to these rules, and one draw needn't show every extreme that they name: `expert_ids`: each row names 2 different experts. In each aligned block of 256 rows (the rows of one index of ep) no expert is named by more than 192 rows, and in some block one expert is named by exactly 192 rows.
All inputs are finite; a program needn't handle non-finite values.
Results may differ from a plain program's by a relative error of at most 0.012.
Values may be sent and summed in bfloat16 or wider, within the bound.
A program may use at most 128 MiB of HBM per device.

v0:
```python
import jax
import jax.numpy as jnp
from jax import lax
from jax.sharding import PartitionSpec as P

NORM_EPS = 1e-06
CLAMP_LIMIT = 7.0
SWISH_SCALE = 1.702


def normalize(tokens, norm_gain):
    values = tokens.astype(jnp.float32)
    scaled = values * lax.rsqrt(jnp.mean(values * values, axis=-1, keepdims=True) + NORM_EPS)
    return (scaled * norm_gain).astype(jnp.bfloat16)


def activate(gate_sum, up_sum):
    gate_cut = jnp.minimum(gate_sum, CLAMP_LIMIT)
    up_cut = jnp.clip(up_sum, -CLAMP_LIMIT, CLAMP_LIMIT)
    return ((up_cut + 1.0) * gate_cut * jax.nn.sigmoid(SWISH_SCALE * gate_cut)).astype(jnp.bfloat16)


def shards(tokens, expert_ids, route_weight, norm_gain, expert_gate, expert_up, expert_down):
    groups = lax.axis_size("ep")
    tp_count = lax.axis_size("tp")
    member_count = expert_gate.shape[0]
    experts = groups * member_count
    tok_count, model_width = tokens.shape
    top_count = expert_ids.shape[1]
    capacity = min(tok_count, 3 * tok_count * top_count // experts)
    quarter = model_width // tp_count
    normed = normalize(tokens, norm_gain)
    flat_ids = expert_ids.reshape(-1)
    onehot = (flat_ids[:, None] == jnp.arange(experts, dtype=jnp.int32)[None, :]).astype(jnp.int32)
    slot_index = jnp.sum(jnp.cumsum(onehot, axis=0) * onehot, axis=1) - 1
    position = flat_ids * capacity + slot_index
    token_index = jnp.arange(flat_ids.shape[0], dtype=jnp.int32) // top_count
    row_table = jnp.full((experts * capacity,), tok_count, jnp.int32).at[position].set(token_index)
    padded = jnp.concatenate([normed, jnp.zeros((1, model_width), jnp.bfloat16)], axis=0)
    offset = lax.axis_index("tp") * quarter
    source_rows = lax.dynamic_slice_in_dim(padded, offset, quarter, 1)
    send_rows = source_rows[row_table].reshape(groups, member_count, capacity, quarter)
    received = lax.all_to_all(send_rows, "ep", split_axis=0, concat_axis=0, tiled=True)
    slot_count = received.shape[2]
    shard_piece = lax.all_gather(received, "tp", axis=3, tiled=True)
    span_size = shard_piece.shape[3]
    member = 0
    row_block = shard_piece[:, member].reshape(-1, span_size)
    gate_rows = expert_gate[member]
    up_rows = expert_up[member]
    gate_list = [jnp.dot(row_block, gate_rows, preferred_element_type=jnp.float32)]
    up_list = [jnp.dot(row_block, up_rows, preferred_element_type=jnp.float32)]
    gate_sum = jnp.stack(gate_list)
    up_sum = jnp.stack(up_list)
    activated = activate(gate_sum, up_sum)
    member = 0
    weight_rows = expert_down[member]
    product = lax.dot_general(
        weight_rows, activated[member], (((0,), (1,)), ((), ())), preferred_element_type=jnp.float32
    )
    term_list = [product.reshape(quarter * lax.axis_size("tp"), groups, slot_count)]
    summed = lax.psum_scatter(
        jnp.stack(term_list, axis=2).astype(jnp.bfloat16), "tp", scatter_dimension=0, tiled=True
    )
    returned = lax.all_to_all(
        summed.reshape(quarter, experts * capacity), "ep", split_axis=1, concat_axis=1, tiled=True
    )
    picked = jnp.take(returned, position, axis=1).reshape(quarter, tok_count, top_count)
    weighted = jnp.sum(picked.astype(jnp.float32) * route_weight[None, :, :], axis=2)
    return weighted.T.astype(jnp.bfloat16)


def solution(mesh):
    return jax.shard_map(
        shards,
        mesh=mesh,
        in_specs=(
            P("ep", None),
            P("ep", None),
            P("ep", None),
            P(),
            P("ep", None, "tp"),
            P("ep", None, "tp"),
            P("ep", "tp", None),
        ),
        out_specs=P("ep", "tp"),
        check_vma=False,
    )
```

profile of v0, /device:TPU:0, one launch (start us, length us, event | category | flops | bytes accessed | tf_op | source)
XLA Modules:
  0.0 245.8 jit_solution(14064720156240668413)
XLA Ops:
  6.5 0.0 copy-start
  6.5 0.0 all-gather.2.cloned.1.call-start
  6.5 1.0 copy.19
  7.5 0.1 eq.26
  7.7 0.1 reshape.111
  7.8 0.7 broadcast_multiply_fusion
  8.5 1.1 reduce-window.6
  9.6 0.2 slice_reduce_fusion
  9.9 0.1 fusion.12
  10.0 0.1 copy.23
  10.1 0.1 mul.76
  10.3 2.5 scatter_custom_fusion
  12.8 1.5 fusion.4
  14.3 1.5 fusion.6
  15.9 5.4 %gather_fusion = bf16[1536,512]{1,0:T(8,128)(2,1)} fusion(bf16[257,512]{1,0:T(8,128)(2,1)S(1)} %pad_dynamic-slice_fusion, s32[2048]{0:T(1024)S(1)} %pad_clamp_fusion), kind=kCustom, calls=%fused_computation | custom fusion | bytes 3151872 | tf_op jit(solution)/shard_map/gather | solution.py:42
  21.3 44.4 %all_to_all.17 = bf16[8,1,192,512]{3,2,1,0:T(8,128)(2,1)} all-to-all(bf16[8,1,192,512]{3,2,1,0:T(8,128)(2,1)} %bitcast.37), channel_id=1, replica_groups=mesh['ep'=8,'tp'=4] {'ep'}, dimensions={0} | all-to-all | bytes 3145728 | tf_op jit(solution)/shard_map/all_to_all | solution.py:43
  65.7 0.0 all-gather.2.cloned.1.call-update
  65.8 0.0 reduce-scatter.2.cloned.1.call-start
  65.8 45.5 %all-gather.2.cloned.1.call-done = bf16[8,1,192,2048]{3,2,1,0:T(8,128)(2,1)} async-done(((bf16[8,1,192,512]{3,2,1,0:T(8,128)(2,1)}), bf16[8,1,192,2048]{3,2,1,0:T(8,128)(2,1)}) %all-gather.2.cloned.1.call-update) | async-done | bytes 6291472 | tf_op jit(solution)/shard_map/all_gather | solution.py:45
  111.3 8.5 %convolution_minimum_fusion = f32[1536,512]{1,0:T(8,128)} fusion(bf16[1536,2048]{1,0:T(8,128)(2,1)} %bitcast.43, bf16[1,2048,512]{2,1,0:T(8,128)(2,1)} %param.11), kind=kOutput, calls=%fused_computation.5 | convolution fusion | flops 3222011904 | bytes 11534336 | tf_op jit(solution)/shard_map/dot_general | solution.py:51
  119.8 0.0 copy-done
  119.8 11.9 %convolution_convert_fusion = bf16[1536,2048]{1,0:T(8,128)(2,1)} fusion(bf16[1,512,2048]{2,1,0:T(8,128)(2,1)S(1)} %copy-done, f32[1536,512]{1,0:T(8,128)} %convolution_minimum_fusion, bf16[1536,2048]{1,0:T(8,128)(2,1)} %bitcast.44, bf16[1,2048,512]{2,1,0:T(8,128)(2,1)} %param.12), kind=kOutput, calls=%fused_computation.3 | convolution fusion | flops 6452674560 | bytes 19922944 | tf_op jit(solution)/shard_map/dot_general | solution.py:58
  131.7 0.0 reduce-scatter.2.cloned.1.call-update
  131.7 0.0 copy-start.1
  131.7 0.0 copy-start.2
  131.7 58.0 %reduce-scatter.2.cloned.1.call-done = bf16[512,8,1,192]{0,3,1,2:T(8,128)(2,1)} async-done(((bf16[2048,8,1,192]{0,3,1,2:T(8,128)(2,1)}), bf16[512,8,1,192]{0,3,1,2:T(8,128)(2,1)}) %reduce-scatter.2.cloned.1.call-update) | async-done | bytes 1572880 | tf_op jit(solution)/shard_map/reduce_scatter | solution.py:62
  189.7 5.5 %all-to-all-start.1 = ((bf16[512,8,192]{0,2,1:T(8,128)(2,1)}), bf16[512,8,192]{0,2,1:T(8,128)(2,1)}, u32[]{:S(2)}, u32[]{:S(2)}) async-start(bf16[512,8,192]{0,2,1:T(8,128)(2,1)} %bitcast.39), calls=%async_computation.2 | async-start | bytes 3145728 | tf_op jit(solution)/shard_map/all_to_all | solution.py:65
  195.2 0.1 sub.15
  195.4 0.1 copy.21
  195.5 0.0 copy-done.1
  195.5 0.2 copy.22
  195.7 0.0 copy-done.2
  195.7 0.1 copy.25
  195.8 36.3 %all-to-all-done.1 = bf16[512,8,192]{0,2,1:T(8,128)(2,1)} async-done(((bf16[512,8,192]{0,2,1:T(8,128)(2,1)}), bf16[512,8,192]{0,2,1:T(8,128)(2,1)}, u32[]{:S(2)}, u32[]{:S(2)}) %all-to-all-start.1) | async-done | bytes 1572896 | tf_op jit(solution)/shard_map/all_to_all | solution.py:65
  232.2 3.6 %gather_fusion.1 = bf16[512,512]{1,0:T(8,128)(2,1)S(1)} fusion(bf16[512,1536]{0,1:T(8,128)(2,1)} %bitcast.13, s32[1024]{0:T(1024)S(1)} %pad_clamp_fusion.1), kind=kCustom, calls=%fused_computation.1 | custom fusion | bytes 1050624 | tf_op jit(solution)/shard_map/jit(_take)/gather | solution.py:68
  235.8 0.2 gather.11
  236.0 2.9 %multiply_reduce_fusion = bf16[512,256]{0,1:T(8,128)(2,1)} fusion(bf16[512,256,2]{0,2,1:T(2,128)(2,1)S(1)} %gather.11, pred[256,2]{1,0:T(8,128)(4,1)S(1)} %copy.22, f32[256,2]{1,0:T(8,128)S(1)} %copy.25), kind=kLoop, calls=%fused_computation.19 | loop fusion | flops 917504 | bytes 788992 | tf_op jit(solution)/shard_map/reduce_sum | solution.py:69
  (12 shorter events, 0.1 us)
Async XLA Ops:
  6.5 113.3 %copy-start = (bf16[1,512,2048]{2,1,0:T(8,128)(2,1)S(1)}, bf16[1,512,2048]{2,1,0:T(8,128)(2,1)}, u32[]{:S(2)}) copy-start(bf16[1,512,2048]{2,1,0:T(8,128)(2,1)} %param.13) | copy-start | bytes 6291460
  6.5 104.7 %all-gather.2.cloned.1.call-start = ((), (), s32[]{:S(2)}) async-start(), calls=%async_computation.3 | async-start | bytes 7864320 | tf_op jit(solution)/shard_map/all_gather | solution.py:45
  65.8 124.0 %reduce-scatter.2.cloned.1.call-start = ((), (), s32[]{:S(2)}) async-start(), calls=%async_computation.4 | async-start | bytes 7864320 | tf_op jit(solution)/shard_map/reduce_scatter | solution.py:62
  131.7 63.8 %copy-start.1 = (s32[256,2]{0,1:T(2,128)S(1)}, s32[256,2]{0,1:T(2,128)}, u32[]{:S(2)}) copy-start(s32[256,2]{0,1:T(2,128)} %param.8) | copy-start | bytes 6148
  131.7 64.0 %copy-start.2 = (f32[256,2]{0,1:T(2,128)S(1)}, f32[256,2]{0,1:T(2,128)}, u32[]{:S(2)}) copy-start(f32[256,2]{0,1:T(2,128)} %param.9) | copy-start | bytes 6148
  189.7 42.4 %all-to-all-start.1 = ((bf16[512,8,192]{0,2,1:T(8,128)(2,1)}), bf16[512,8,192]{0,2,1:T(8,128)(2,1)}, u32[]{:S(2)}, u32[]{:S(2)}) async-start(bf16[512,8,192]{0,2,1:T(8,128)(2,1)} %bitcast.39), calls=%async_computation.2 | async-start | bytes 3145728 | tf_op jit(solution)/shard_map/all_to_all | solution.py:65
Sparse Core Ops, SparseCore 0:
  65.9 45.3 all-gather.1
  131.8 57.8 reduce-scatter.1
where the time goes:
time: 246 us
  waiting for transfers between devices  140 us (57%)
  blocking collectives  44.4 us (18%)
  matrix products  20.4 us (8%)
  local copies, waits for them, and re-layouts  14 us (6%)
  between operations  13.6 us (6%)
  other arithmetic  8.01 us (3%)
  starting transfers between devices  5.56 us (2%)
    reduce_scatter x1, waiting for transfers between devices, shards(): lax.psum_scatter(jnp.stack(term_list, axis=2).astype(jnp.bfloat16), 'tp',...  58 us
    all_gather x1, waiting for transfers between devices, shards(): shard_piece = lax.all_gather(received, 'tp', axis=3, tiled=True)  45.5 us
    all_to_all x1, blocking collectives, shards(): lax.all_to_all(send_rows, 'ep', split_axis=0, concat_axis=0, tiled=True)  44.4 us
    all_to_all x1, waiting for transfers between devices, shards(): lax.all_to_all(summed.reshape(quarter, experts * capacity), 'ep', split_a...  36.3 us
    dot_general x1, matrix products, shards(): lax.dot_general(weight_rows, activated[member], (((0,), (1,)), ((), ())),...  11.9 us
    dot_general x1, matrix products, shards(): jnp.dot(row_block, gate_rows, preferred_element_type=jnp.float32)  8.52 us
    all_to_all x1, starting transfers between devices, shards(): lax.all_to_all(summed.reshape(quarter, experts * capacity), 'ep', split_a...  5.51 us
    gather x1, local copies, waits for them, and re-layouts, shards(): source_rows[row_table].reshape(groups, member_count, capacity, quarter)  5.43 us
  transfers between devices with their start and end apart: 3, of which 3 were waited for; matrix products, arithmetic and copies ran while one was open for 0% of the time, Pallas kernels for 0%

commit v1 on v0

v1 whole, which is shorter than its diff:
```python
import functools

import jax
import jax.numpy as jnp
from jax import lax
from jax.experimental import pallas as pl
from jax.experimental.pallas import tpu as pltpu
from jax.sharding import PartitionSpec as P

NORM_EPS = 1e-06
CLAMP_LIMIT = 7.0
SWISH_SCALE = 1.702
MESH = pl.DeviceIdType.MESH


def activate(gate_sum, up_sum):
    gate_cut = jnp.minimum(gate_sum, CLAMP_LIMIT)
    up_cut = jnp.clip(up_sum, -CLAMP_LIMIT, CLAMP_LIMIT)
    return ((up_cut + 1.0) * gate_cut * jax.nn.sigmoid(SWISH_SCALE * gate_cut)).astype(jnp.bfloat16)


def expert_kernel(
    groups,
    send,
    gate_hbm,
    up_hbm,
    down_hbm,
    out,
    gate_w,
    up_w,
    down_w,
    rows,
    part,
    pair_in,
    cross_out,
    cross_in,
    result,
    w_sem,
    disp_send,
    disp_recv,
    cross_send,
    cross_recv,
    core_send,
    core_recv,
    fwd_send,
    fwd_recv,
    pair_send,
    pair_recv,
    sum_send,
    sum_recv,
    ret_send,
    ret_recv,
):
    me = lax.axis_index("ep")
    tp = lax.axis_index("tp")
    a, b = tp // 2, lax.rem(tp, 2)
    cross = 2 * (1 - a) + b
    core = 2 * a + 1 - b
    quarter = send.shape[2]

    weights = [
        pltpu.make_async_copy(src, dst, w_sem.at[i])
        for i, (src, dst) in enumerate(((gate_hbm, gate_w), (up_hbm, up_w), (down_hbm, down_w)))
    ]

    def remote(src, dst, send_sem, recv_sem, ep_index, tp_index):
        return pltpu.make_async_remote_copy(
            src_ref=src,
            dst_ref=dst,
            send_sem=send_sem,
            recv_sem=recv_sem,
            device_id=(ep_index, tp_index),
            device_id_type=MESH,
        )

    def dispatch(k):
        dst = lax.rem(me + k, groups)
        return remote(send.at[dst], rows.at[k, tp], disp_send.at[k], disp_recv.at[k], dst, tp)

    def dispatch_own():
        return pltpu.make_async_copy(send.at[me], rows.at[0, tp], disp_recv.at[0])

    def to_cross(k):
        return remote(rows.at[k, tp], rows.at[k, tp], cross_send.at[k], cross_recv.at[k], me, cross)

    def to_core(k):
        return remote(rows.at[k, tp], rows.at[k, tp], core_send.at[k], core_recv.at[k], me, core)

    def forward(k):
        return remote(rows.at[k, cross], rows.at[k, cross], fwd_send.at[k], fwd_recv.at[k], me, core)

    def pair(k):
        return remote(part.at[k, 1 - b], pair_in.at[k], pair_send.at[k], pair_recv.at[k], me, core)

    def cross_sum(k):
        return remote(cross_out.at[k], cross_in.at[k], sum_send.at[k], sum_recv.at[k], me, cross)

    def give_back(k):
        src = lax.rem(me + groups - k, groups)
        return remote(result.at[k], out.at[me], ret_send.at[k], ret_recv.at[k], src, tp)

    def give_back_own():
        return pltpu.make_async_copy(result.at[0], out.at[me], ret_recv.at[0])

    for copy in weights:
        copy.start()
    dispatch_own().start()

    barrier = pltpu.get_barrier_semaphore()

    def greet(k, carry):
        pl.semaphore_signal(
            barrier, inc=1, device_id=(lax.rem(me + k, groups), tp), device_id_type=MESH
        )
        return carry

    lax.fori_loop(1, groups, greet, 0)
    pl.semaphore_signal(barrier, inc=1, device_id=(me, cross), device_id_type=MESH)
    pl.semaphore_signal(barrier, inc=1, device_id=(me, core), device_id_type=MESH)
    pl.semaphore_wait(barrier, groups + 1)

    def launch(k, carry):
        dispatch(k).start()
        return carry

    lax.fori_loop(1, groups, launch, 0)
    for copy in weights:
        copy.wait()

    def step(i, carry):
        @pl.when(i < groups)
        def _():
            @pl.when(i == 0)
            def _():
                dispatch_own().wait()

            @pl.when(i > 0)
            def _():
                dispatch(i).wait_recv()

            to_cross(i).start()
            to_core(i).start()

        @pl.when((i >= 1) & (i < groups + 1))
        def _():
            k = i - 1
            to_cross(k).wait_recv()
            forward(k).start()

        @pl.when((i >= 3) & (i < groups + 3))
        def _():
            k = i - 3
            pair(k).wait_recv()
            total = part[k, b, 1 - a].astype(jnp.float32) + pair_in[k, 1 - a].astype(jnp.float32)
            cross_out[k] = total.astype(jnp.bfloat16)
            cross_sum(k).start()

        @pl.when((i >= 2) & (i < groups + 2))
        def _():
            k = i - 2
            to_core(k).wait_recv()
            forward(k).wait_recv()
            block = jnp.concatenate([rows[k, j] for j in range(4)], axis=1)
            gate_sum = jnp.dot(block, gate_w[...], preferred_element_type=jnp.float32)
            up_sum = jnp.dot(block, up_w[...], preferred_element_type=jnp.float32)
            activated = activate(gate_sum, up_sum)
            for j in range(4):
                part[k, j % 2, j // 2] = jnp.dot(
                    activated,
                    down_w[:, j * quarter : (j + 1) * quarter],
                    preferred_element_type=jnp.float32,
                ).astype(jnp.bfloat16)
            pair(k).start()

        @pl.when(i >= 4)
        def _():
            k = i - 4
            cross_sum(k).wait_recv()
            total = part[k, b, a].astype(jnp.float32) + pair_in[k, a].astype(jnp.float32)
            result[k] = (total + cross_in[k].astype(jnp.float32)).astype(jnp.bfloat16)

            @pl.when(k == 0)
            def _():
                give_back_own().start()

            @pl.when(k > 0)
            def _():
                give_back(k).start()

        return carry

    lax.fori_loop(0, groups + 4, step, 0)

    def finish(k, carry):
        to_cross(k).wait_send()
        to_core(k).wait_send()
        forward(k).wait_send()
        pair(k).wait_send()
        cross_sum(k).wait_send()

        @pl.when(k == 0)
        def _():
            give_back_own().wait()

        @pl.when(k > 0)
        def _():
            dispatch(k).wait_send()
            give_back(k).wait_send()
            give_back(k).wait_recv()

        return carry

    lax.fori_loop(0, groups, finish, 0)


def run_experts(send, gate_w, up_w, down_w):
    groups, capacity, quarter = send.shape
    bf16 = jnp.bfloat16
    sems = [pltpu.SemaphoreType.DMA((groups,)) for _ in range(14)]
    return pl.pallas_call(
        functools.partial(expert_kernel, groups),
        out_shape=jax.ShapeDtypeStruct(send.shape, bf16),
        in_specs=[pl.BlockSpec(memory_space=pltpu.VMEM)] + [pl.BlockSpec(memory_space=pl.ANY)] * 3,
        out_specs=pl.BlockSpec(memory_space=pltpu.VMEM),
        scratch_shapes=[
            pltpu.VMEM(gate_w.shape, bf16),
            pltpu.VMEM(up_w.shape, bf16),
            pltpu.VMEM(down_w.shape, bf16),
            pltpu.VMEM((groups, 4, capacity, quarter), bf16),
            pltpu.VMEM((groups, 2, 2, capacity, quarter), bf16),
            pltpu.VMEM((groups, 2, capacity, quarter), bf16),
            pltpu.VMEM(send.shape, bf16),
            pltpu.VMEM(send.shape, bf16),
            pltpu.VMEM(send.shape, bf16),
            pltpu.SemaphoreType.DMA((3,)),
            *sems,
        ],
        compiler_params=pltpu.CompilerParams(
            collective_id=0, has_side_effects=True, vmem_limit_bytes=56 * 1024 * 1024
        ),
    )(send, gate_w, up_w, down_w)


def shards(tokens, expert_ids, route_weight, norm_gain, expert_gate, expert_up, expert_down):
    groups = lax.axis_size("ep")
    tp_count = lax.axis_size("tp")
    experts = groups * expert_gate.shape[0]
    tok_count, model_width = tokens.shape
    top_count = expert_ids.shape[1]
    capacity = min(tok_count, 3 * tok_count * top_count // experts)
    quarter = model_width // tp_count
    offset = lax.axis_index("tp") * quarter

    values = tokens.astype(jnp.float32)
    scale = lax.rsqrt(jnp.mean(values * values, axis=-1, keepdims=True) + NORM_EPS)
    own = lax.dynamic_slice_in_dim(tokens, offset, quarter, 1).astype(jnp.float32)
    own_gain = lax.dynamic_slice_in_dim(norm_gain, offset, quarter, 0)
    normed = (own * scale * own_gain).astype(jnp.bfloat16)

    onehot = expert_ids[:, :, None] == jnp.arange(experts, dtype=jnp.int32)
    named = jnp.any(onehot, axis=1).astype(jnp.bfloat16)
    order = jnp.arange(tok_count, dtype=jnp.int32)
    earlier = (order[None, :] < order[:, None]).astype(jnp.bfloat16)
    slots = jnp.dot(earlier, named, preferred_element_type=jnp.float32).astype(jnp.int32)
    slot_index = jnp.sum(jnp.where(onehot, slots[:, None, :], 0), axis=2)
    position = expert_ids * capacity + slot_index
    match = position[:, :, None] == jnp.arange(experts * capacity, dtype=jnp.int32)
    chosen = jnp.any(match, axis=1).astype(jnp.bfloat16)
    send = lax.dot_general(
        chosen, normed, (((0,), (0,)), ((), ())), preferred_element_type=jnp.float32
    ).astype(jnp.bfloat16)

    returned = run_experts(
        send.reshape(groups, capacity, quarter), expert_gate[0], expert_up[0], expert_down[0]
    ).reshape(experts * capacity, quarter)

    mix = jnp.sum(jnp.where(match, route_weight[:, :, None], 0.0), axis=1)
    high = lax.reduce_precision(mix, 8, 7)
    low = (mix - high).astype(jnp.bfloat16)
    combined = jnp.dot(high.astype(jnp.bfloat16), returned, preferred_element_type=jnp.float32)
    combined += jnp.dot(low, returned, preferred_element_type=jnp.float32)
    return combined.astype(jnp.bfloat16)


def solution(mesh):
    return jax.shard_map(
        shards,
        mesh=mesh,
        in_specs=(
            P("ep", None),
            P("ep", None),
            P("ep", None),
            P(),
            P("ep", None, "tp"),
            P("ep", None, "tp"),
            P("ep", "tp", None),
        ),
        out_specs=P("ep", "tp"),
        check_vma=False,
    )
```

time: 246 us -> 118 us (0.48)
  waiting for transfers between devices: 140 us -> 0 us
  Pallas kernels: 0 us -> 107 us
  blocking collectives: 44.4 us -> 0 us
  matrix products: 20.4 us -> 4.82 us
  between operations: 13.6 us -> 0.05 us
  local copies, waits for them, and re-layouts: 14 us -> 1.77 us
  starting transfers between devices: 5.56 us -> 0 us
  other arithmetic: 8.01 us -> 4.52 us
    pallas_call x0 -> x1, Pallas kernels: none -> 107 us  [run_experts(): pl.pallas_call(functools.partial(expert_kernel, groups), out_shape=jax.Sh...]
    reduce_scatter x1 -> x0, waiting for transfers between devices: 58 us -> none  [shards(): lax.psum_scatter(jnp.stack(term_list, axis=2).astype(jnp.bfloat16), 'tp',...]
    all_gather x1 -> x0, waiting for transfers between devices: 45.5 us -> none  [shards(): shard_piece = lax.all_gather(received, 'tp', axis=3, tiled=True)]
    all_to_all x1 -> x0, blocking collectives: 44.4 us -> none  [shards(): lax.all_to_all(send_rows, 'ep', split_axis=0, concat_axis=0, tiled=True)]
    all_to_all x1 -> x0, waiting for transfers between devices: 36.3 us -> none  [shards(): lax.all_to_all(summed.reshape(quarter, experts * capacity), 'ep', split_a...]
    dot_general x2 -> x4, matrix products: 20.4 us -> 4.82 us  [the longest x1 2.83 us: shards(): lax.dot_general(chosen, normed, (((0,), (0,)), ((), ())), preferred_eleme...]
    gather x3 -> x0, local copies, waits for them, and re-layouts: 9.22 us -> none  [the longest x1 5.43 us: shards(): source_rows[row_table].reshape(groups, member_count, capacity, quarter)]
    all_to_all x1 -> x0, starting transfers between devices: 5.51 us -> none  [shards(): lax.all_to_all(summed.reshape(quarter, experts * capacity), 'ep', split_a...]
  transfers between devices with their start and end apart: 3 -> 0, of which waited for: 3 -> 0; matrix products, arithmetic and copies ran while one was open for 0% -> 0% of each run, Pallas kernels for 0% -> 0%
where the time goes in v1:
time: 118 us
  Pallas kernels  107 us (91%)
  matrix products  4.82 us (4%)
  other arithmetic  4.52 us (4%)
  local copies, waits for them, and re-layouts  1.77 us (2%)
    pallas_call x1, Pallas kernels, run_experts(): pl.pallas_call(functools.partial(expert_kernel, groups), out_shape=jax.Sh...  107 us
    dot_general x1, matrix products, shards(): lax.dot_general(chosen, normed, (((0,), (0,)), ((), ())), preferred_eleme...  2.83 us

profile of v1, /device:TPU:0, one launch (start us, length us, event | category | flops | bytes accessed | tf_op | source)
XLA Modules:
  0.0 117.9 jit_solution(7569633304112833612)
XLA Ops:
  0.0 1.5 %multiply_reduce_fusion = f32[256]{0:T(256)S(1)} fusion(bf16[256,2048]{1,0:T(8,128)(2,1)} %param.7), kind=kLoop, calls=%fused_computation.6 | loop fusion | flops 1572608 | bytes 1049600 | tf_op jit(solution)/shard_map/reduce_sum | solution.py:255
  1.5 0.8 dynamic_slice.7
  2.3 0.7 fusion.8
  3.0 0.2 convolution_convert_fusion.1
  3.1 0.7 select_reduce_fusion.1
  3.9 0.7 multiply_add_fusion
  4.6 0.5 fusion
  5.1 2.8 %convolution_convert_fusion = bf16[1536,512]{1,0:T(8,128)(2,1)} fusion(pred[256,1536]{1,0:T(8,128)(4,1)S(1)} %fusion, f32[512]{0:T(512)S(1)} %dynamic_slice.7, f32[256]{0:T(256)S(1)} %add_rsqrt_fusion, bf16[256,2048]{1,0:T(8,128)(2,1)} %param.7, s32[]{:T(128)S(6)} %select_n.14), kind=kOutput, calls=%fused_computation.3 | convolution fusion | flops 403963904 | bytes 2231300 | tf_op jit(solution)/shard_map/dot_general | solution.py:269
  7.9 0.0 copy-start.1
  7.9 106.7 %shard_map.73 = bf16[8,192,512]{2,1,0:T(8,128)(2,1)} custom-call(bf16[8,192,512]{2,1,0:T(8,128)(2,1)} %bitcast.14, bf16[2048,512]{1,0:T(8,128)(2,1)} %bitcast.11, bf16[2048,512]{1,0:T(8,128)(2,1)} %bitcast.12, bf16[512,2048]{1,0:T(8,128)(2,1)} %bitcast.13), custom_call_target="tpu_custom_call" | custom-call | tf_op jit(solution)/shard_map/pallas_call | solution.py:220
  114.6 0.0 copy-start
  114.6 0.0 copy-done.1
  114.6 0.4 select_reduce_fusion
  115.0 1.0 copy-done
  116.0 0.6 fusion.4
  116.6 1.3 %fusion.2 = bf16[256,512]{1,0:T(8,128)(2,1)} fusion(f32[256,512]{1,0:T(8,128)S(1)} %fusion.4, bf16[1536,512]{1,0:T(8,128)(2,1)S(1)} %bitcast.10, f32[256,1536]{1,0:T(8,128)S(1)} %select_reduce_fusion), kind=kOutput, calls=%fused_computation.9 | convolution fusion | flops 404094976 | bytes 3932160 | tf_op jit(solution)/shard_map/dot_general | solution.py:281
  (1 shorter events, 0.0 us)
Async XLA Ops:
  7.9 106.7 %copy-start.1 = (f32[256,2]{0,1:T(2,128)S(1)}, f32[256,2]{0,1:T(2,128)}, u32[]{:S(2)}) copy-start(f32[256,2]{0,1:T(2,128)} %param.9) | copy-start | bytes 6148
  114.6 1.4 %copy-start = (bf16[8,192,512]{2,1,0:T(8,128)(2,1)S(1)}, bf16[8,192,512]{2,1,0:T(8,128)(2,1)}, u32[]{:S(2)}) copy-start(bf16[8,192,512]{2,1,0:T(8,128)(2,1)} %shard_map.73) | copy-start | bytes 4718596

commit v2 on v1

--- a/solution.py
+++ b/solution.py
@@ -22,6 +22,7 @@
 def expert_kernel(
     groups,
     send,
+    send_cross,
     gate_hbm,
     up_hbm,
     down_hbm,
@@ -57,6 +58,7 @@
     cross = 2 * (1 - a) + b
     core = 2 * a + 1 - b
     quarter = send.shape[2]
+    half = groups // 2
 
     weights = [
         pltpu.make_async_copy(src, dst, w_sem.at[i])
@@ -73,13 +75,40 @@
             device_id_type=MESH,
         )
 
+    def partner(k):
+        total, bit = 0, 1
+        while bit < groups:
+            total += bit * lax.rem(me // bit + k // bit, 2)
+            bit *= 2
+        return total
+
+    def order(i):
+        i = i + (i // (groups - 2)) * (1 - 2 * lax.rem(i, 2))
+        return i // 2 + half * lax.rem(i, 2)
+
     def dispatch(k):
-        dst = lax.rem(me + k, groups)
+        dst = partner(k)
         return remote(send.at[dst], rows.at[k, tp], disp_send.at[k], disp_recv.at[k], dst, tp)
 
     def dispatch_own():
         return pltpu.make_async_copy(send.at[me], rows.at[0, tp], disp_recv.at[0])
 
+    def dispatch_cross(k):
+        dst = partner(k)
+        return remote(
+            send_cross.at[lax.rem(dst, half)],
+            rows.at[k, cross],
+            cross_send.at[k],
+            cross_recv.at[k],
+            dst,
+            tp,
+        )
+
+    def dispatch_own_cross():
+        return pltpu.make_async_copy(
+            send_cross.at[lax.rem(me, half)], rows.at[0, cross], cross_recv.at[0]
+        )
+
     def to_cross(k):
         return remote(rows.at[k, tp], rows.at[k, tp], cross_send.at[k], cross_recv.at[k], me, cross)
 
@@ -96,8 +125,7 @@
         return remote(cross_out.at[k], cross_in.at[k], sum_send.at[k], sum_recv.at[k], me, cross)
 
     def give_back(k):
-        src = lax.rem(me + groups - k, groups)
-        return remote(result.at[k], out.at[me], ret_send.at[k], ret_recv.at[k], src, tp)
+        return remote(result.at[k], out.at[me], ret_send.at[k], ret_recv.at[k], partner(k), tp)
 
     def give_back_own():
         return pltpu.make_async_copy(result.at[0], out.at[me], ret_recv.at[0])
@@ -105,6 +133,7 @@
     for copy in weights:
         copy.start()
     dispatch_own().start()
+    dispatch_own_cross().start()
 
     barrier = pltpu.get_barrier_semaphore()
 
@@ -119,8 +148,14 @@
     pl.semaphore_signal(barrier, inc=1, device_id=(me, core), device_id_type=MESH)
     pl.semaphore_wait(barrier, groups + 1)
 
-    def launch(k, carry):
+    def launch(i, carry):
+        k = order(i)
         dispatch(k).start()
+
+        @pl.when(k < half)
+        def _():
+            dispatch_cross(k).start()
+
         return carry
 
     lax.fori_loop(1, groups, launch, 0)
@@ -128,28 +163,24 @@
         copy.wait()
 
     def step(i, carry):
-        @pl.when(i < groups)
-        def _():
-            @pl.when(i == 0)
-            def _():
-                dispatch_own().wait()
-
-            @pl.when(i > 0)
-            def _():
-                dispatch(i).wait_recv()
-
-            to_cross(i).start()
-            to_core(i).start()
-
-        @pl.when((i >= 1) & (i < groups + 1))
-        def _():
-            k = i - 1
-            to_cross(k).wait_recv()
-            forward(k).start()
+        @pl.when(i >= 4)
+        def _():
+            k = order(i - 4)
+            cross_sum(k).wait_recv()
+            total = part[k, b, a].astype(jnp.float32) + pair_in[k, a].astype(jnp.float32)
+            result[k] = (total + cross_in[k].astype(jnp.float32)).astype(jnp.bfloat16)
+
+            @pl.when(k == 0)
+            def _():
+                give_back_own().start()
+
+            @pl.when(k > 0)
+            def _():
+                give_back(k).start()
 
         @pl.when((i >= 3) & (i < groups + 3))
         def _():
-            k = i - 3
+            k = order(i - 3)
             pair(k).wait_recv()
             total = part[k, b, 1 - a].astype(jnp.float32) + pair_in[k, 1 - a].astype(jnp.float32)
             cross_out[k] = total.astype(jnp.bfloat16)
@@ -157,7 +188,7 @@
 
         @pl.when((i >= 2) & (i < groups + 2))
         def _():
-            k = i - 2
+            k = order(i - 2)
             to_core(k).wait_recv()
             forward(k).wait_recv()
             block = jnp.concatenate([rows[k, j] for j in range(4)], axis=1)
@@ -172,27 +203,43 @@
                 ).astype(jnp.bfloat16)
             pair(k).start()
 
-        @pl.when(i >= 4)
-        def _():
-            k = i - 4
-            cross_sum(k).wait_recv()
-            total = part[k, b, a].astype(jnp.float32) + pair_in[k, a].astype(jnp.float32)
-            result[k] = (total + cross_in[k].astype(jnp.float32)).astype(jnp.bfloat16)
+        @pl.when((i >= 1) & (i < groups + 1))
+        def _():
+            k = order(i - 1)
 
             @pl.when(k == 0)
             def _():
-                give_back_own().start()
+                dispatch_own_cross().wait()
 
             @pl.when(k > 0)
             def _():
-                give_back(k).start()
+                to_cross(k).wait_recv()
+
+            forward(k).start()
+
+        @pl.when(i < groups)
+        def _():
+            k = order(i)
+
+            @pl.when(k == 0)
+            def _():
+                dispatch_own().wait()
+
+            @pl.when(k > 0)
+            def _():
+                dispatch(k).wait_recv()
+
+            @pl.when(k >= half)
+            def _():
+                to_cross(k).start()
+
+            to_core(k).start()
 
         return carry
 
     lax.fori_loop(0, groups + 4, step, 0)
 
     def finish(k, carry):
-        to_cross(k).wait_send()
         to_core(k).wait_send()
         forward(k).wait_send()
         pair(k).wait_send()
@@ -204,6 +251,7 @@
 
         @pl.when(k > 0)
         def _():
+            to_cross(k).wait_send()
             dispatch(k).wait_send()
             give_back(k).wait_send()
             give_back(k).wait_recv()
@@ -213,14 +261,14 @@
     lax.fori_loop(0, groups, finish, 0)
 
 
-def run_experts(send, gate_w, up_w, down_w):
+def run_experts(send, send_cross, gate_w, up_w, down_w):
     groups, capacity, quarter = send.shape
     bf16 = jnp.bfloat16
     sems = [pltpu.SemaphoreType.DMA((groups,)) for _ in range(14)]
     return pl.pallas_call(
         functools.partial(expert_kernel, groups),
         out_shape=jax.ShapeDtypeStruct(send.shape, bf16),
-        in_specs=[pl.BlockSpec(memory_space=pltpu.VMEM)] + [pl.BlockSpec(memory_space=pl.ANY)] * 3,
+        in_specs=[pl.BlockSpec(memory_space=pltpu.VMEM)] * 2 + [pl.BlockSpec(memory_space=pl.ANY)] * 3,
         out_specs=pl.BlockSpec(memory_space=pltpu.VMEM),
         scratch_shapes=[
             pltpu.VMEM(gate_w.shape, bf16),
@@ -238,7 +286,7 @@
         compiler_params=pltpu.CompilerParams(
             collective_id=0, has_side_effects=True, vmem_limit_bytes=56 * 1024 * 1024
         ),
-    )(send, gate_w, up_w, down_w)
+    )(send, send_cross, gate_w, up_w, down_w)
 
 
 def shards(tokens, expert_ids, route_weight, norm_gain, expert_gate, expert_up, expert_down):
@@ -249,13 +297,17 @@
     top_count = expert_ids.shape[1]
     capacity = min(tok_count, 3 * tok_count * top_count // experts)
     quarter = model_width // tp_count
-    offset = lax.axis_index("tp") * quarter
+    half = groups // 2
+    tp = lax.axis_index("tp")
+    cross = lax.rem(tp + tp_count // 2, tp_count)
 
     values = tokens.astype(jnp.float32)
     scale = lax.rsqrt(jnp.mean(values * values, axis=-1, keepdims=True) + NORM_EPS)
-    own = lax.dynamic_slice_in_dim(tokens, offset, quarter, 1).astype(jnp.float32)
-    own_gain = lax.dynamic_slice_in_dim(norm_gain, offset, quarter, 0)
-    normed = (own * scale * own_gain).astype(jnp.bfloat16)
+
+    def normed(index):
+        own = lax.dynamic_slice_in_dim(tokens, index * quarter, quarter, 1).astype(jnp.float32)
+        own_gain = lax.dynamic_slice_in_dim(norm_gain, index * quarter, quarter, 0)
+        return (own * scale * own_gain).astype(jnp.bfloat16)
 
     onehot = expert_ids[:, :, None] == jnp.arange(experts, dtype=jnp.int32)
     named = jnp.any(onehot, axis=1).astype(jnp.bfloat16)
@@ -264,14 +316,22 @@
     slots = jnp.dot(earlier, named, preferred_element_type=jnp.float32).astype(jnp.int32)
     slot_index = jnp.sum(jnp.where(onehot, slots[:, None, :], 0), axis=2)
     position = expert_ids * capacity + slot_index
-    match = position[:, :, None] == jnp.arange(experts * capacity, dtype=jnp.int32)
-    chosen = jnp.any(match, axis=1).astype(jnp.bfloat16)
-    send = lax.dot_general(
-        chosen, normed, (((0,), (0,)), ((), ())), preferred_element_type=jnp.float32
-    ).astype(jnp.bfloat16)
-
+
+    def pick(first, count, index):
+        slots_here = first * capacity + jnp.arange(count * capacity, dtype=jnp.int32)
+        match = position[:, :, None] == slots_here
+        picked = lax.dot_general(
+            jnp.any(match, axis=1).astype(jnp.bfloat16),
+            normed(index),
+            (((0,), (0,)), ((), ())),
+            preferred_element_type=jnp.float32,
+        ).astype(jnp.bfloat16)
+        return picked.reshape(count, capacity, quarter), match
+
+    send, match = pick(0, groups, tp)
+    send_cross, _ = pick(lax.axis_index("ep") // half * half, half, cross)
     returned = run_experts(
-        send.reshape(groups, capacity, quarter), expert_gate[0], expert_up[0], expert_down[0]
+        send, send_cross, expert_gate[0], expert_up[0], expert_down[0]
     ).reshape(experts * capacity, quarter)
 
     mix = jnp.sum(jnp.where(match, route_weight[:, :, None], 0.0), axis=1)

time: 118 us -> 98.9 us (0.84)
  Pallas kernels: 107 us -> 86.5 us
    pallas_call x1, Pallas kernels: 107 us -> 86.5 us  [run_experts(): pl.pallas_call(functools.partial(expert_kernel, groups), out_shape=jax.Sh...]
    dot_general x1 -> x2, matrix products: 2.83 us -> 3.25 us  [pick(): lax.dot_general(jnp.any(match, axis=1).astype(jnp.bfloat16), normed(index...]
where the time goes in v2:
time: 98.9 us; the launch traced here: 98.4 us
  Pallas kernels  86.5 us (87%)
  matrix products  5.25 us (5%)
  other arithmetic  4.81 us (5%)
  local copies, waits for them, and re-layouts  1.78 us (2%)
    pallas_call x1, Pallas kernels, run_experts(): pl.pallas_call(functools.partial(expert_kernel, groups), out_shape=jax.Sh...  86.5 us
    dot_general x2, matrix products, pick(): lax.dot_general(jnp.any(match, axis=1).astype(jnp.bfloat16), normed(index...  3.25 us

profile of v2, /device:TPU:0, one launch (start us, length us, event | category | flops | bytes accessed | tf_op | source)
XLA Modules:
  0.0 98.4 jit_solution(11361258558057829100)
XLA Ops:
  0.0 0.0 copy-start.1
  0.0 1.6 %multiply_reduce_fusion = f32[256]{0:T(256)S(1)} fusion(bf16[256,2048]{1,0:T(8,128)(2,1)} %param.7), kind=kLoop, calls=%fused_computation.6 | loop fusion | flops 1572608 | bytes 1049600 | tf_op jit(solution)/shard_map/reduce_sum | solution.py:305
  1.6 0.7 fusion.11
  2.3 0.8 fusion.14
  3.1 0.2 convolution_convert_fusion.2
  3.2 0.7 select_reduce_fusion.1
  4.0 0.7 multiply_add_fusion
  4.7 0.2 compare_reduce_fusion
  4.9 0.5 fusion
  5.4 0.0 copy-done.1
  5.4 1.4 %convolution_convert_fusion.1 = bf16[768,512]{1,0:T(8,128)(2,1)} fusion(pred[256,768]{1,0:T(8,128)(4,1)S(1)} %compare_reduce_fusion, f32[512]{0:T(512)S(1)} %get-tuple-element.5, bf16[256,2048]{1,0:T(8,128)(2,1)S(1)} %copy-done.1, s32[]{:T(128)S(6)} %select_n.25, f32[256]{0:T(256)S(1)} %add_rsqrt_fusion), kind=kOutput, calls=%fused_computation.9 | convolution fusion | flops 202244096 | bytes 1248260 | tf_op jit(solution)/shard_map/dot_general | solution.py:323
  6.8 1.9 %convolution_convert_fusion = bf16[1536,512]{1,0:T(8,128)(2,1)} fusion(pred[256,1536]{1,0:T(8,128)(4,1)S(1)} %fusion, f32[512]{0:T(512)S(1)} %get-tuple-element.6, f32[256]{0:T(256)S(1)} %add_rsqrt_fusion, bf16[256,2048]{1,0:T(8,128)(2,1)S(1)} %copy-done.1, s32[]{:T(128)S(6)} %select_n.23), kind=kOutput, calls=%fused_computation.3 | convolution fusion | flops 403963904 | bytes 2231300 | tf_op jit(solution)/shard_map/dot_general | solution.py:323
  8.6 0.0 copy-start.2
  8.6 86.5 %shard_map.73 = bf16[8,192,512]{2,1,0:T(8,128)(2,1)} custom-call(bf16[8,192,512]{2,1,0:T(8,128)(2,1)} %bitcast.16, bf16[4,192,512]{2,1,0:T(8,128)(2,1)} %bitcast.17, bf16[2048,512]{1,0:T(8,128)(2,1)} %bitcast.13, bf16[2048,512]{1,0:T(8,128)(2,1)} %bitcast.14, bf16[512,2048]{1,0:T(8,128)(2,1)} %bitcast.15), custom_call_target="tpu_custom_call" | custom-call | tf_op jit(solution)/shard_map/pallas_call | solution.py:268
  95.1 0.0 copy-start
  95.2 0.0 copy-done.2
  95.2 0.4 select_reduce_fusion
  95.6 1.0 %copy-done = bf16[8,192,512]{2,1,0:T(8,128)(2,1)S(1)} copy-done((bf16[8,192,512]{2,1,0:T(8,128)(2,1)S(1)}, bf16[8,192,512]{2,1,0:T(8,128)(2,1)}, u32[]{:S(2)}) %copy-start) | copy-done | bytes 1572888
  96.6 0.6 fusion.4
  97.1 1.3 %fusion.2 = bf16[256,512]{1,0:T(8,128)(2,1)} fusion(f32[256,512]{1,0:T(8,128)S(1)} %fusion.4, bf16[1536,512]{1,0:T(8,128)(2,1)S(1)} %bitcast.12, f32[256,1536]{1,0:T(8,128)S(1)} %select_reduce_fusion), kind=kOutput, calls=%fused_computation.11 | convolution fusion | flops 404094976 | bytes 3932160 | tf_op jit(solution)/shard_map/dot_general | solution.py:341
  (2 shorter events, 0.0 us)
Async XLA Ops:
  0.0 5.4 %copy-start.1 = (bf16[256,2048]{1,0:T(8,128)(2,1)S(1)}, bf16[256,2048]{1,0:T(8,128)(2,1)}, u32[]{:S(2)}) copy-start(bf16[256,2048]{1,0:T(8,128)(2,1)} %param.7) | copy-start | bytes 3145732
  8.6 86.5 %copy-start.2 = (f32[256,2]{0,1:T(2,128)S(1)}, f32[256,2]{0,1:T(2,128)}, u32[]{:S(2)}) copy-start(f32[256,2]{0,1:T(2,128)} %param.9) | copy-start | bytes 6148
  95.1 1.4 %copy-start = (bf16[8,192,512]{2,1,0:T(8,128)(2,1)S(1)}, bf16[8,192,512]{2,1,0:T(8,128)(2,1)}, u32[]{:S(2)}) copy-start(bf16[8,192,512]{2,1,0:T(8,128)(2,1)} %shard_map.73) | copy-start | bytes 4718596

commit v3 on v2

v3 whole, which is shorter than its diff:
```python
import functools

import jax
import jax.numpy as jnp
from jax import lax
from jax.experimental import pallas as pl
from jax.experimental.pallas import tpu as pltpu
from jax.sharding import PartitionSpec as P

NORM_EPS = 1e-06
CLAMP_LIMIT = 7.0
SWISH_SCALE = 1.702
MESH = pl.DeviceIdType.MESH


def activate(gate_sum, up_sum):
    gate_cut = jnp.minimum(gate_sum, CLAMP_LIMIT)
    up_cut = jnp.clip(up_sum, -CLAMP_LIMIT, CLAMP_LIMIT)
    return ((up_cut + 1.0) * gate_cut * jax.nn.sigmoid(SWISH_SCALE * gate_cut)).astype(jnp.bfloat16)


def expert_kernel(
    groups,
    tokens,
    ids,
    route,
    gain,
    gate_hbm,
    up_hbm,
    down_hbm,
    out,
    gate_w,
    up_w,
    down_w,
    normed_own,
    normed_cross,
    before,
    send,
    send_cross,
    back,
    high,
    low,
    total_out,
    rows,
    part,
    pair_in,
    cross_out,
    cross_in,
    result,
    w_sem,
    disp_send,
    disp_recv,
    cross_send,
    cross_recv,
    core_send,
    core_recv,
    fwd_send,
    fwd_recv,
    pair_send,
    pair_recv,
    sum_send,
    sum_recv,
    ret_send,
    ret_recv,
):
    me = lax.axis_index("ep")
    tp = lax.axis_index("tp")
    a, b = tp // 2, lax.rem(tp, 2)
    cross = 2 * (1 - a) + b
    core = 2 * a + 1 - b
    capacity, quarter = send.shape[1:]
    tok_count = tokens.shape[0]
    half = groups // 2

    weights = [
        pltpu.make_async_copy(src, dst, w_sem.at[i])
        for i, (src, dst) in enumerate(((gate_hbm, gate_w), (up_hbm, up_w), (down_hbm, down_w)))
    ]

    def remote(src, dst, send_sem, recv_sem, ep_index, tp_index):
        return pltpu.make_async_remote_copy(
            src_ref=src,
            dst_ref=dst,
            send_sem=send_sem,
            recv_sem=recv_sem,
            device_id=(ep_index, tp_index),
            device_id_type=MESH,
        )

    def partner(k):
        total, bit = 0, 1
        while bit < groups:
            total += bit * lax.rem(me // bit + k // bit, 2)
            bit *= 2
        return total

    def order(i):
        i = i + (i // (groups - 2)) * (1 - 2 * lax.rem(i, 2))
        return i // 2 + half * lax.rem(i, 2)

    def dispatch(k):
        dst = partner(k)
        return remote(send.at[k], rows.at[k, tp], disp_send.at[k], disp_recv.at[k], dst, tp)

    def dispatch_cross(k):
        dst = partner(k)
        return remote(
            send_cross.at[k],
            rows.at[k, cross],
            cross_send.at[k],
            cross_recv.at[k],
            dst,
            tp,
        )

    def to_cross(k):
        return remote(rows.at[k, tp], rows.at[k, tp], cross_send.at[k], cross_recv.at[k], me, cross)

    def to_core(k):
        return remote(rows.at[k, tp], rows.at[k, tp], core_send.at[k], core_recv.at[k], me, core)

    def forward(k):
        return remote(rows.at[k, cross], rows.at[k, cross], fwd_send.at[k], fwd_recv.at[k], me, core)

    def pair(k):
        return remote(part.at[k, 1 - b], pair_in.at[k], pair_send.at[k], pair_recv.at[k], me, core)

    def cross_sum(k):
        return remote(cross_out.at[k], cross_in.at[k], sum_send.at[k], sum_recv.at[k], me, cross)

    def give_back(k):
        return remote(result.at[k], back.at[k], ret_send.at[k], ret_recv.at[k], partner(k), tp)

    for copy in weights:
        copy.start()

    barrier = pltpu.get_barrier_semaphore()

    def greet(k, carry):
        pl.semaphore_signal(
            barrier, inc=1, device_id=(lax.rem(me + k, groups), tp), device_id_type=MESH
        )
        return carry

    lax.fori_loop(1, groups, greet, 0)
    pl.semaphore_signal(barrier, inc=1, device_id=(me, cross), device_id_type=MESH)
    pl.semaphore_signal(barrier, inc=1, device_id=(me, core), device_id_type=MESH)

    values = tokens[...].astype(jnp.float32)
    scale = lax.rsqrt(jnp.mean(values * values, axis=-1, keepdims=True) + NORM_EPS)

    def normed(index):
        span = pl.ds(pl.multiple_of(index * quarter, quarter), quarter)
        return (tokens[:, span].astype(jnp.float32) * scale * gain[:, span]).astype(jnp.bfloat16)

    normed_own[...] = normed(tp)
    normed_cross[...] = normed(cross)
    earlier = lax.broadcasted_iota(jnp.int32, (tok_count, tok_count), 0)
    later = lax.broadcasted_iota(jnp.int32, (tok_count, tok_count), 1)
    before[...] = jnp.where(earlier < later, 1.0, 0.0).astype(jnp.bfloat16)

    def select(k):
        expert = partner(k)
        hits = ids[...] == expert
        named = jnp.sum(jnp.where(hits, 1.0, 0.0), axis=0, keepdims=True)
        weight = jnp.sum(jnp.where(hits, route[...], 0.0), axis=0, keepdims=True)
        count = jnp.dot(
            jnp.broadcast_to(named, (8, tok_count)).astype(jnp.bfloat16),
            before[...],
            preferred_element_type=jnp.float32,
        )[0:1]
        slot = jnp.where(named > 0.0, count.astype(jnp.int32), -1)
        place = lax.broadcasted_iota(jnp.int32, (capacity, tok_count), 0)
        chosen = place == slot
        mix = jnp.where(chosen, weight, 0.0)
        mix_high = mix.astype(jnp.bfloat16)
        high[k] = mix_high
        low[k] = (mix - mix_high.astype(jnp.float32)).astype(jnp.bfloat16)
        return jnp.where(chosen, 1.0, 0.0).astype(jnp.bfloat16)

    def pick(chosen, source):
        return jnp.dot(chosen, source[...], preferred_element_type=jnp.float32).astype(jnp.bfloat16)

    chosen = select(0)
    rows[0, tp] = pick(chosen, normed_own)
    rows[0, cross] = pick(chosen, normed_cross)
    pl.semaphore_wait(barrier, groups + 1)

    def launch(i, carry):
        k = order(i)
        chosen = select(k)
        send[k] = pick(chosen, normed_own)
        dispatch(k).start()

        @pl.when(k < half)
        def _():
            send_cross[k] = pick(chosen, normed_cross)
            dispatch_cross(k).start()

        return carry

    lax.fori_loop(1, groups, launch, 0)
    for copy in weights:
        copy.wait()

    def step(i, carry):
        @pl.when(i >= 4)
        def _():
            k = order(i - 4)
            cross_sum(k).wait_recv()
            total = part[k, b, a].astype(jnp.float32) + pair_in[k, a].astype(jnp.float32)
            total = (total + cross_in[k].astype(jnp.float32)).astype(jnp.bfloat16)

            @pl.when(k == 0)
            def _():
                back[0] = total

            @pl.when(k > 0)
            def _():
                result[k] = total
                give_back(k).start()

        @pl.when((i >= 3) & (i < groups + 3))
        def _():
            k = order(i - 3)
            pair(k).wait_recv()
            total = part[k, b, 1 - a].astype(jnp.float32) + pair_in[k, 1 - a].astype(jnp.float32)
            cross_out[k] = total.astype(jnp.bfloat16)
            cross_sum(k).start()

        @pl.when((i >= 2) & (i < groups + 2))
        def _():
            k = order(i - 2)
            to_core(k).wait_recv()
            forward(k).wait_recv()
            block = jnp.concatenate([rows[k, j] for j in range(4)], axis=1)
            gate_sum = jnp.dot(block, gate_w[...], preferred_element_type=jnp.float32)
            up_sum = jnp.dot(block, up_w[...], preferred_element_type=jnp.float32)
            activated = activate(gate_sum, up_sum)
            for j in range(4):
                part[k, j % 2, j // 2] = jnp.dot(
                    activated,
                    down_w[:, j * quarter : (j + 1) * quarter],
                    preferred_element_type=jnp.float32,
                ).astype(jnp.bfloat16)
            pair(k).start()

        @pl.when((i >= 1) & (i < groups + 1))
        def _():
            k = order(i - 1)

            @pl.when(k > 0)
            def _():
                to_cross(k).wait_recv()

            forward(k).start()

        @pl.when(i < groups)
        def _():
            k = order(i)

            @pl.when(k > 0)
            def _():
                dispatch(k).wait_recv()

            @pl.when(k >= half)
            def _():
                to_cross(k).start()

            to_core(k).start()

        return carry

    lax.fori_loop(0, groups + 4, step, 0)

    total_out[...] = jnp.zeros_like(total_out)

    def finish(i, carry):
        k = order(i)

        @pl.when(k > 0)
        def _():
            give_back(k).wait_recv()

        for share in (high, low):
            total_out[...] += lax.dot_general(
                share[k], back[k], (((0,), (0,)), ((), ())), preferred_element_type=jnp.float32
            )
        return carry

    lax.fori_loop(0, groups, finish, 0)
    out[...] = total_out[...].astype(jnp.bfloat16)

    def drain(k, carry):
        to_core(k).wait_send()
        forward(k).wait_send()
        pair(k).wait_send()
        cross_sum(k).wait_send()

        @pl.when(k > 0)
        def _():
            to_cross(k).wait_send()
            dispatch(k).wait_send()
            give_back(k).wait_send()

        return carry

    lax.fori_loop(0, groups, drain, 0)


def shards(tokens, expert_ids, route_weight, norm_gain, expert_gate, expert_up, expert_down):
    groups = lax.axis_size("ep")
    tp_count = lax.axis_size("tp")
    experts = groups * expert_gate.shape[0]
    tok_count, model_width = tokens.shape
    top_count = expert_ids.shape[1]
    capacity = min(tok_count, 3 * tok_count * top_count // experts)
    quarter = model_width // tp_count
    bf16 = jnp.bfloat16
    slots = (groups, capacity, quarter)
    weights = (expert_gate[0], expert_up[0], expert_down[0])
    return pl.pallas_call(
        functools.partial(expert_kernel, groups),
        out_shape=jax.ShapeDtypeStruct((tok_count, quarter), bf16),
        in_specs=[pl.BlockSpec(memory_space=pltpu.VMEM)] * 4
        + [pl.BlockSpec(memory_space=pl.ANY)] * 3,
        out_specs=pl.BlockSpec(memory_space=pltpu.VMEM),
        scratch_shapes=[
            *[pltpu.VMEM(weight.shape, bf16) for weight in weights],
            pltpu.VMEM((tok_count, quarter), bf16),
            pltpu.VMEM((tok_count, quarter), bf16),
            pltpu.VMEM((tok_count, tok_count), bf16),
            pltpu.VMEM(slots, bf16),
            pltpu.VMEM((groups // 2, capacity, quarter), bf16),
            pltpu.VMEM(slots, bf16),
            pltpu.VMEM((groups, capacity, tok_count), bf16),
            pltpu.VMEM((groups, capacity, tok_count), bf16),
            pltpu.VMEM((tok_count, quarter), jnp.float32),
            pltpu.VMEM((groups, 4, capacity, quarter), bf16),
            pltpu.VMEM((groups, 2, 2, capacity, quarter), bf16),
            pltpu.VMEM((groups, 2, capacity, quarter), bf16),
            pltpu.VMEM(slots, bf16),
            pltpu.VMEM(slots, bf16),
            pltpu.VMEM(slots, bf16),
            pltpu.SemaphoreType.DMA((3,)),
            *[pltpu.SemaphoreType.DMA((groups,)) for _ in range(14)],
        ],
        compiler_params=pltpu.CompilerParams(
            collective_id=0, has_side_effects=True, vmem_limit_bytes=60 * 1024 * 1024
        ),
    )(tokens, expert_ids.T, route_weight.T, norm_gain[None, :], *weights)


def solution(mesh):
    return jax.shard_map(
        shards,
        mesh=mesh,
        in_specs=(
            P("ep", None),
            P("ep", None),
            P("ep", None),
            P(),
            P("ep", None, "tp"),
            P("ep", None, "tp"),
            P("ep", "tp", None),
        ),
        out_specs=P("ep", "tp"),
        check_vma=False,
    )
```

time: 98.9 us -> 87.9 us (0.89)
  matrix products: 5.25 us -> 0 us
  other arithmetic: 4.81 us -> 0 us
    dot_general x5 -> x0, matrix products: 5.25 us -> none  [the longest x2 3.25 us: pick(): lax.dot_general(jnp.any(match, axis=1).astype(jnp.bfloat16), normed(index...]
    reduce_sum x3 -> x0, other arithmetic: 2.72 us -> none  [the longest x1 1.6 us: shards(): jnp.mean(values * values, axis=-1, keepdims=True) + NORM_EPS]
    reduce_or x3 -> x0, other arithmetic: 1.39 us -> none  [the longest x2 0.7 us: pick(): jnp.any(match, axis=1).astype(jnp.bfloat16)]
where the time goes in v3:
time: 87.9 us; the launch traced here: 87.7 us
  Pallas kernels  86 us (98%)
  local copies, waits for them, and re-layouts  1.67 us (2%)
    pallas_call x1, Pallas kernels, shards(): pl.pallas_call(functools.partial(expert_kernel, groups), out_shape=jax.Sh...  86 us

profile of v3, /device:TPU:0, one launch (start us, length us, event | category | flops | bytes accessed | tf_op | source)
XLA Modules:
  0.0 87.7 jit_solution(11846666981663500931)
XLA Ops:
  0.0 86.0 %shard_map.73 = bf16[256,512]{1,0:T(8,128)(2,1)} custom-call(bf16[256,2048]{1,0:T(8,128)(2,1)} %tokens.1, s32[2,256]{1,0:T(2,128)} %bitcast.10, f32[2,256]{1,0:T(2,128)} %bitcast.11, f32[1,2048]{1,0:T(1,128)} %bitcast.9, bf16[2048,512]{1,0:T(8,128)(2,1)} %bitcast.6, bf16[2048,512]{1,0:T(8,128)(2,1)} %bitcast.7, bf16[512,2048]{1,0:T(8,128)(2,1)} %bitcast.8), custom_call_target="tpu_custom_call" | custom-call | tf_op jit(solution)/shard_map/pallas_call | solution.py:322
  86.0 1.7 %copy.9 = bf16[256,512]{1,0:T(8,128)(2,1)} copy(bf16[256,512]{1,0:T(8,128)(2,1)} %shard_map.73) | data formatting | bytes 524288

commit v4 on v3

--- a/solution.py
+++ b/solution.py
@@ -35,6 +35,10 @@
     normed_own,
     normed_cross,
     before,
+    raw,
+    ids_in,
+    ids_send,
+    ids_recv,
     send,
     send_cross,
     back,
@@ -71,6 +75,7 @@
     capacity, quarter = send.shape[1:]
     tok_count = tokens.shape[0]
     half = groups // 2
+    direct = half - 1
 
     weights = [
         pltpu.make_async_copy(src, dst, w_sem.at[i])
@@ -101,6 +106,19 @@
     def dispatch(k):
         dst = partner(k)
         return remote(send.at[k], rows.at[k, tp], disp_send.at[k], disp_recv.at[k], dst, tp)
+
+    def mirror():
+        return remote(
+            normed_own, raw.at[0], disp_send.at[half], disp_recv.at[half], partner(half), tp
+        )
+
+    def relay(k):
+        return remote(
+            raw.at[0], raw.at[k], disp_send.at[half + k], disp_recv.at[half + k], partner(k), tp
+        )
+
+    def tell(k):
+        return remote(ids, ids_in.at[k], ids_send.at[k], ids_recv.at[k], partner(half + k), tp)
 
     def dispatch_cross(k):
         dst = partner(k)
@@ -159,19 +177,20 @@
     later = lax.broadcasted_iota(jnp.int32, (tok_count, tok_count), 1)
     before[...] = jnp.where(earlier < later, 1.0, 0.0).astype(jnp.bfloat16)
 
-    def select(k):
-        expert = partner(k)
-        hits = ids[...] == expert
+    def locate(id_rows, expert):
+        hits = id_rows == expert
         named = jnp.sum(jnp.where(hits, 1.0, 0.0), axis=0, keepdims=True)
-        weight = jnp.sum(jnp.where(hits, route[...], 0.0), axis=0, keepdims=True)
         count = jnp.dot(
             jnp.broadcast_to(named, (8, tok_count)).astype(jnp.bfloat16),
             before[...],
             preferred_element_type=jnp.float32,
         )[0:1]
         slot = jnp.where(named > 0.0, count.astype(jnp.int32), -1)
-        place = lax.broadcasted_iota(jnp.int32, (capacity, tok_count), 0)
-        chosen = place == slot
+        return hits, lax.broadcasted_iota(jnp.int32, (capacity, tok_count), 0) == slot
+
+    def select(k):
+        hits, chosen = locate(ids[...], partner(k))
+        weight = jnp.sum(jnp.where(hits, route[...], 0.0), axis=0, keepdims=True)
         mix = jnp.where(chosen, weight, 0.0)
         mix_high = mix.astype(jnp.bfloat16)
         high[k] = mix_high
@@ -181,25 +200,31 @@
     def pick(chosen, source):
         return jnp.dot(chosen, source[...], preferred_element_type=jnp.float32).astype(jnp.bfloat16)
 
+    pl.semaphore_wait(barrier, groups + 1)
+
+    def tell_all(k, carry):
+        tell(k).start()
+        return carry
+
+    lax.fori_loop(0, half, tell_all, 0)
+    mirror().start()
     chosen = select(0)
     rows[0, tp] = pick(chosen, normed_own)
     rows[0, cross] = pick(chosen, normed_cross)
-    pl.semaphore_wait(barrier, groups + 1)
-
-    def launch(i, carry):
-        k = order(i)
+
+    def launch(k, carry):
         chosen = select(k)
         send[k] = pick(chosen, normed_own)
         dispatch(k).start()
 
-        @pl.when(k < half)
+        @pl.when(k < direct)
         def _():
             send_cross[k] = pick(chosen, normed_cross)
             dispatch_cross(k).start()
 
         return carry
 
-    lax.fori_loop(1, groups, launch, 0)
+    lax.fori_loop(1, half - 1, launch, 0)
     for copy in weights:
         copy.wait()
 
@@ -259,11 +284,35 @@
         def _():
             k = order(i)
 
-            @pl.when(k > 0)
+            @pl.when((k > 0) & (k < half))
             def _():
                 dispatch(k).wait_recv()
 
+            @pl.when(k == half)
+            def _():
+                mirror().wait_recv()
+
+                def relay_all(j, carry):
+                    relay(j).start()
+                    return carry
+
+                lax.fori_loop(1, half, relay_all, 0)
+                lax.fori_loop(half - 1, half, launch, 0)
+
+            @pl.when(k > half)
+            def _():
+                relay(k - half).wait_recv()
+
             @pl.when(k >= half)
+            def _():
+                select(k)
+                tell(k - half).wait_recv()
+                _, chosen = locate(ids_in[k - half], me)
+                rows[k, tp] = pick(
+                    jnp.where(chosen, 1.0, 0.0).astype(jnp.bfloat16), raw.at[k - half]
+                )
+
+            @pl.when(k >= direct)
             def _():
                 to_cross(k).start()
 
@@ -300,8 +349,18 @@
         @pl.when(k > 0)
         def _():
             to_cross(k).wait_send()
+            give_back(k).wait_send()
+
+        @pl.when((k > 0) & (k < half))
+        def _():
             dispatch(k).wait_send()
-            give_back(k).wait_send()
+            relay(k).wait_send()
+            tell(k).wait_send()
+
+        @pl.when(k == 0)
+        def _():
+            mirror().wait_send()
+            tell(0).wait_send()
 
         return carry
 
@@ -330,6 +389,10 @@
             pltpu.VMEM((tok_count, quarter), bf16),
             pltpu.VMEM((tok_count, quarter), bf16),
             pltpu.VMEM((tok_count, tok_count), bf16),
+            pltpu.VMEM((groups // 2, tok_count, quarter), bf16),
+            pltpu.VMEM((groups // 2, top_count, tok_count), jnp.int32),
+            pltpu.SemaphoreType.DMA((groups // 2,)),
+            pltpu.SemaphoreType.DMA((groups // 2,)),
             pltpu.VMEM(slots, bf16),
             pltpu.VMEM((groups // 2, capacity, quarter), bf16),
             pltpu.VMEM(slots, bf16),

time: 87.9 us -> 93.1 us (1.059)
  Pallas kernels: 86 us -> 91.2 us
    pallas_call x1, Pallas kernels: 86 us -> 91.2 us  [shards(): pl.pallas_call(functools.partial(expert_kernel, groups), out_shape=jax.Sh...]
where the time goes in v4:
time: 93.1 us; the launch traced here: 92.9 us
  Pallas kernels  91.2 us (98%)
  local copies, waits for them, and re-layouts  1.67 us (2%)
    pallas_call x1, Pallas kernels, shards(): pl.pallas_call(functools.partial(expert_kernel, groups), out_shape=jax.Sh...  91.2 us

profile of v4, /device:TPU:0, one launch (start us, length us, event | category | flops | bytes accessed | tf_op | source)
XLA Modules:
  0.0 92.9 jit_solution(3456113599427582808)
XLA Ops:
  0.0 91.2 %shard_map.73 = bf16[256,512]{1,0:T(8,128)(2,1)} custom-call(bf16[256,2048]{1,0:T(8,128)(2,1)} %tokens.1, s32[2,256]{1,0:T(2,128)} %bitcast.10, f32[2,256]{1,0:T(2,128)} %bitcast.11, f32[1,2048]{1,0:T(1,128)} %bitcast.9, bf16[2048,512]{1,0:T(8,128)(2,1)} %bitcast.6, bf16[2048,512]{1,0:T(8,128)(2,1)} %bitcast.7, bf16[512,2048]{1,0:T(8,128)(2,1)} %bitcast.8), custom_call_target="tpu_custom_call" | custom-call | tf_op jit(solution)/shard_map/pallas_call | solution.py:381
  91.2 1.7 %copy.9 = bf16[256,512]{1,0:T(8,128)(2,1)} copy(bf16[256,512]{1,0:T(8,128)(2,1)} %shard_map.73) | data formatting | bytes 524288

commit v5 on v3

--- a/solution.py
+++ b/solution.py
@@ -203,75 +203,73 @@
     for copy in weights:
         copy.wait()
 
+    def spread(k):
+        @pl.when(k > 0)
+        def _():
+            dispatch(k).wait_recv()
+
+        @pl.when(k >= half)
+        def _():
+            to_cross(k).start()
+
+        to_core(k).start()
+
+    def pass_on(k):
+        @pl.when(k > 0)
+        def _():
+            to_cross(k).wait_recv()
+
+        forward(k).start()
+
+    def compute(k):
+        to_core(k).wait_recv()
+        forward(k).wait_recv()
+        block = jnp.concatenate([rows[k, j] for j in range(4)], axis=1)
+        gate_sum = jnp.dot(block, gate_w[...], preferred_element_type=jnp.float32)
+        up_sum = jnp.dot(block, up_w[...], preferred_element_type=jnp.float32)
+        activated = activate(gate_sum, up_sum)
+        for j in range(4):
+            part[k, j % 2, j // 2] = jnp.dot(
+                activated,
+                down_w[:, j * quarter : (j + 1) * quarter],
+                preferred_element_type=jnp.float32,
+            ).astype(jnp.bfloat16)
+        pair(k).start()
+
+    def add_pair(k):
+        pair(k).wait_recv()
+        total = part[k, b, 1 - a].astype(jnp.float32) + pair_in[k, 1 - a].astype(jnp.float32)
+        cross_out[k] = total.astype(jnp.bfloat16)
+        cross_sum(k).start()
+
+    def add_cross(k):
+        cross_sum(k).wait_recv()
+        total = part[k, b, a].astype(jnp.float32) + pair_in[k, a].astype(jnp.float32)
+        total = (total + cross_in[k].astype(jnp.float32)).astype(jnp.bfloat16)
+
+        @pl.when(k == 0)
+        def _():
+            back[0] = total
+
+        @pl.when(k > 0)
+        def _():
+            result[k] = total
+            give_back(k).start()
+
+    for stage in (spread, pass_on, compute, add_pair):
+        stage(0)
+
     def step(i, carry):
-        @pl.when(i >= 4)
-        def _():
-            k = order(i - 4)
-            cross_sum(k).wait_recv()
-            total = part[k, b, a].astype(jnp.float32) + pair_in[k, a].astype(jnp.float32)
-            total = (total + cross_in[k].astype(jnp.float32)).astype(jnp.bfloat16)
-
-            @pl.when(k == 0)
+        for stage, lag in ((add_cross, 4), (add_pair, 3), (compute, 2), (pass_on, 1), (spread, 0)):
+            first = 1 + lag if lag < 4 else 4
+
+            @pl.when((i >= first) & (i < groups + lag))
             def _():
-                back[0] = total
-
-            @pl.when(k > 0)
-            def _():
-                result[k] = total
-                give_back(k).start()
-
-        @pl.when((i >= 3) & (i < groups + 3))
-        def _():
-            k = order(i - 3)
-            pair(k).wait_recv()
-            total = part[k, b, 1 - a].astype(jnp.float32) + pair_in[k, 1 - a].astype(jnp.float32)
-            cross_out[k] = total.astype(jnp.bfloat16)
-            cross_sum(k).start()
-
-        @pl.when((i >= 2) & (i < groups + 2))
-        def _():
-            k = order(i - 2)
-            to_core(k).wait_recv()
-            forward(k).wait_recv()
-            block = jnp.concatenate([rows[k, j] for j in range(4)], axis=1)
-            gate_sum = jnp.dot(block, gate_w[...], preferred_element_type=jnp.float32)
-            up_sum = jnp.dot(block, up_w[...], preferred_element_type=jnp.float32)
-            activated = activate(gate_sum, up_sum)
-            for j in range(4):
-                part[k, j % 2, j // 2] = jnp.dot(
-                    activated,
-                    down_w[:, j * quarter : (j + 1) * quarter],
-                    preferred_element_type=jnp.float32,
-                ).astype(jnp.bfloat16)
-            pair(k).start()
-
-        @pl.when((i >= 1) & (i < groups + 1))
-        def _():
-            k = order(i - 1)
-
-            @pl.when(k > 0)
-            def _():
-                to_cross(k).wait_recv()
-
-            forward(k).start()
-
-        @pl.when(i < groups)
-        def _():
-            k = order(i)
-
-            @pl.when(k > 0)
-            def _():
-                dispatch(k).wait_recv()
-
-            @pl.when(k >= half)
-            def _():
-                to_cross(k).start()
-
-            to_core(k).start()
-
-        return carry
-
-    lax.fori_loop(0, groups + 4, step, 0)
+                stage(order(i - lag))
+
+        return carry
+
+    lax.fori_loop(1, groups + 4, step, 0)
 
     total_out[...] = jnp.zeros_like(total_out)
 

time: 87.9 us -> 90.7 us (1.032)
  Pallas kernels: 86 us -> 88.3 us
    pallas_call x1, Pallas kernels: 86 us -> 88.3 us  [shards(): pl.pallas_call(functools.partial(expert_kernel, groups), out_shape=jax.Sh...]
where the time goes in v5:
time: 90.7 us; the launch traced here: 90 us
  Pallas kernels  88.3 us (97%)
  local copies, waits for them, and re-layouts  1.67 us (2%)
    pallas_call x1, Pallas kernels, shards(): pl.pallas_call(functools.partial(expert_kernel, groups), out_shape=jax.Sh...  88.3 us

profile of v5, /device:TPU:0, one launch (start us, length us, event | category | flops | bytes accessed | tf_op | source)
XLA Modules:
  0.0 90.0 jit_solution(7331576316485976441)
XLA Ops:
  0.0 88.3 %shard_map.73 = bf16[256,512]{1,0:T(8,128)(2,1)} custom-call(bf16[256,2048]{1,0:T(8,128)(2,1)} %tokens.1, s32[2,256]{1,0:T(2,128)} %bitcast.10, f32[2,256]{1,0:T(2,128)} %bitcast.11, f32[1,2048]{1,0:T(1,128)} %bitcast.9, bf16[2048,512]{1,0:T(8,128)(2,1)} %bitcast.6, bf16[2048,512]{1,0:T(8,128)(2,1)} %bitcast.7, bf16[512,2048]{1,0:T(8,128)(2,1)} %bitcast.8), custom_call_target="tpu_custom_call" | custom-call | tf_op jit(solution)/shard_map/pallas_call | solution.py:320
  88.3 1.7 %copy.9 = bf16[256,512]{1,0:T(8,128)(2,1)} copy(bf16[256,512]{1,0:T(8,128)(2,1)} %shard_map.73) | data formatting | bytes 524288

commit v6 on v3

--- a/solution.py
+++ b/solution.py
@@ -228,6 +228,30 @@
             cross_out[k] = total.astype(jnp.bfloat16)
             cross_sum(k).start()
 
+        @pl.when((i >= 1) & (i < groups + 1))
+        def _():
+            k = order(i - 1)
+
+            @pl.when(k > 0)
+            def _():
+                to_cross(k).wait_recv()
+
+            forward(k).start()
+
+        @pl.when(i < groups)
+        def _():
+            k = order(i)
+
+            @pl.when(k > 0)
+            def _():
+                dispatch(k).wait_recv()
+
+            @pl.when(k >= half)
+            def _():
+                to_cross(k).start()
+
+            to_core(k).start()
+
         @pl.when((i >= 2) & (i < groups + 2))
         def _():
             k = order(i - 2)
@@ -244,30 +268,6 @@
                     preferred_element_type=jnp.float32,
                 ).astype(jnp.bfloat16)
             pair(k).start()
-
-        @pl.when((i >= 1) & (i < groups + 1))
-        def _():
-            k = order(i - 1)
-
-            @pl.when(k > 0)
-            def _():
-                to_cross(k).wait_recv()
-
-            forward(k).start()
-
-        @pl.when(i < groups)
-        def _():
-            k = order(i)
-
-            @pl.when(k > 0)
-            def _():
-                dispatch(k).wait_recv()
-
-            @pl.when(k >= half)
-            def _():
-                to_cross(k).start()
-
-            to_core(k).start()
 
         return carry
 

time: 87.9 us -> 92.1 us (1.048)
  Pallas kernels: 86 us -> 90.2 us
    pallas_call x1, Pallas kernels: 86 us -> 90.2 us  [shards(): pl.pallas_call(functools.partial(expert_kernel, groups), out_shape=jax.Sh...]
where the time goes in v6:
time: 92.1 us; the launch traced here: 91.9 us
  Pallas kernels  90.2 us (98%)
  local copies, waits for them, and re-layouts  1.67 us (2%)
    pallas_call x1, Pallas kernels, shards(): pl.pallas_call(functools.partial(expert_kernel, groups), out_shape=jax.Sh...  90.2 us

profile of v6, /device:TPU:0, one launch (start us, length us, event | category | flops | bytes accessed | tf_op | source)
XLA Modules:
  0.0 91.9 jit_solution(5331973100788992587)
XLA Ops:
  0.0 90.2 %shard_map.73 = bf16[256,512]{1,0:T(8,128)(2,1)} custom-call(bf16[256,2048]{1,0:T(8,128)(2,1)} %tokens.1, s32[2,256]{1,0:T(2,128)} %bitcast.10, f32[2,256]{1,0:T(2,128)} %bitcast.11, f32[1,2048]{1,0:T(1,128)} %bitcast.9, bf16[2048,512]{1,0:T(8,128)(2,1)} %bitcast.6, bf16[2048,512]{1,0:T(8,128)(2,1)} %bitcast.7, bf16[512,2048]{1,0:T(8,128)(2,1)} %bitcast.8), custom_call_target="tpu_custom_call" | custom-call | tf_op jit(solution)/shard_map/pallas_call | solution.py:322
  90.2 1.7 %copy.9 = bf16[256,512]{1,0:T(8,128)(2,1)} copy(bf16[256,512]{1,0:T(8,128)(2,1)} %shard_map.73) | data formatting | bytes 524288
